TPU v7x, 32 devices: a whole 2x2x4 slice. The times are simulated.
32 devices in a mesh: rep: 4 (over z), fs: 4 (over y, x), tp: 2 (over core).
Axes of the slice: x: 2, y: 2, z: 4, core: 2. Of those that a mesh axis runs over, the one named last changes fastest.
Arguments:
- tokens: bfloat16 [2048, 1024], P(('rep', 'fs', 'tp')), may hold values from -6 to 6
- cotangent: bfloat16 [2048, 1024], P(('rep', 'fs', 'tp')), may hold values from -6 to 6
- gate_weight: bfloat16 [1024, 2816], P('fs', 'tp'), may hold values from -0.1875 to 0.1875
- up_weight: bfloat16 [1024, 2816], P('fs', 'tp'), may hold values from -0.1875 to 0.1875
- down_weight: bfloat16 [2816, 1024], P('tp', 'fs'), may hold values from -0.109375 to 0.109375
Outputs:
- input_grad: bfloat16 [2048, 1024], P(('rep', 'fs', 'tp'))
- gate_grad: float32 [1024, 2816], P('fs', 'tp')
- up_grad: float32 [1024, 2816], P('fs', 'tp')
- down_grad: float32 [2816, 1024], P('tp', 'fs')
- gate_power: float32 [1024], P('fs')
- up_power: float32 [1024], P('fs')
- down_power: float32 [2816], P('tp')
All inputs are finite; a program needn't handle non-finite values.
Results may differ from a plain program's by a relative error of at most 0.0017.
Values may be sent and summed in bfloat16 or wider, within the bound.
A program may use at most 64 MiB of HBM per device.

v0:
```python
import math
import jax
import jax.numpy as jnp
from jax import lax
from jax.sharding import PartitionSpec as P

D = 1024
FF = 2816
EPSILON = 1e-06


def contract_rows(left, right):
    return lax.dot_general(
        left, right, (((0,), (0,)), ((), ())), preferred_element_type=jnp.float32
    )


def contract_cols(left, right):
    return lax.dot_general(
        left, right, (((1,), (1,)), ((), ())), preferred_element_type=jnp.float32
    )


def on_device(tokens, cotangent, gate_weight, up_weight, down_weight):
    tp_count = lax.axis_size("tp")
    fs_count = lax.axis_size("fs")
    rep_count = lax.axis_size("rep")
    width = tokens.shape[1]
    factor = 1.0 / math.sqrt(tokens.shape[0] * tp_count * fs_count * rep_count)
    xfloat = tokens.astype(jnp.float32)
    recip_norm = lax.rsqrt(jnp.mean(xfloat * xfloat, axis=1, keepdims=True) + EPSILON)
    normed_exact = xfloat * recip_norm
    normed = normed_exact.astype(jnp.bfloat16)
    group_normed, group_cotangent = (
        lax.all_gather(normed, "tp", axis=0, tiled=True),
        lax.all_gather(cotangent, "tp", axis=0, tiled=True),
    )
    gate_full, up_full, down_full = (
        lax.all_gather(gate_weight, "fs", axis=0, tiled=True),
        lax.all_gather(up_weight, "fs", axis=0, tiled=True),
        lax.all_gather(down_weight.T, "fs", axis=0, tiled=True),
    )
    gate_pre = jnp.dot(group_normed, gate_full, preferred_element_type=jnp.float32)
    up_pre = jnp.dot(group_normed, up_full, preferred_element_type=jnp.float32)
    sigmoid_gate = jax.nn.sigmoid(gate_pre)
    activated = gate_pre * sigmoid_gate
    hidden = (activated * up_pre).astype(jnp.bfloat16)
    grad_hidden = 0.5 * jnp.dot(group_cotangent, down_full, preferred_element_type=jnp.float32)
    grad_up_pre = (grad_hidden * activated).astype(jnp.bfloat16)
    grad_gate_pre = (
        grad_hidden * up_pre * sigmoid_gate * (1.0 + gate_pre * (1.0 - sigmoid_gate))
    ).astype(jnp.bfloat16)
    normed_part = contract_cols(grad_gate_pre, gate_full) + contract_cols(grad_up_pre, up_full)
    grad_normed = lax.psum_scatter(normed_part, "tp", scatter_dimension=0, tiled=True)
    inner = jnp.mean(grad_normed * normed_exact, axis=1, keepdims=True)
    input_grad = (recip_norm * (grad_normed - normed_exact * inner)).astype(jnp.bfloat16)
    hidden_local = gate_weight.shape[1]

    def rows_term():
        normed_cols = lax.slice_in_dim(
            group_normed, 0, width // fs_count * lax.axis_size("fs"), axis=1
        )
        cotangent_cols = lax.slice_in_dim(
            group_cotangent, 0, width // fs_count * lax.axis_size("fs"), axis=1
        )
        return factor * jnp.concatenate(
            [
                contract_rows(normed_cols, grad_gate_pre),
                contract_rows(normed_cols, grad_up_pre),
                0.5 * contract_rows(cotangent_cols, hidden),
            ],
            axis=1,
        )

    reduced = lax.psum_scatter(rows_term(), "fs", scatter_dimension=0, tiled=True)
    reduced = lax.psum(reduced, "rep")
    gate_grad = reduced[:, :hidden_local]
    up_grad = reduced[:, hidden_local : 2 * hidden_local]
    down_grad = reduced[:, 2 * hidden_local :].T
    gate_sums, up_sums = lax.psum(
        (jnp.sum(gate_grad * gate_grad, axis=1), jnp.sum(up_grad * up_grad, axis=1)), "tp"
    )
    down_sums = lax.psum(jnp.sum(down_grad * down_grad, axis=1), "fs")
    return (input_grad, gate_grad, up_grad, down_grad, gate_sums / FF, up_sums / FF, down_sums / D)


def solution(mesh):
    placed = (
        P(("rep", "fs", "tp"), None),
        P(("rep", "fs", "tp"), None),
        P("fs", "tp"),
        P("fs", "tp"),
        P("tp", "fs"),
    )
    return jax.shard_map(
        on_device,
        mesh=mesh,
        in_specs=placed,
        out_specs=(
            P(("rep", "fs", "tp"), None),
            P("fs", "tp"),
            P("fs", "tp"),
            P("tp", "fs"),
            P("fs"),
            P("fs"),
            P("tp"),
        ),
        check_vma=False,
    )
```

profile of v0, /device:TPU:0, one launch (start us, length us, event | category | flops | bytes accessed | tf_op | source)
XLA Modules:
  0.0 513.0 jit_solution(5771994517067918810)
XLA Ops:
  7.2 0.0 copy-start.5
  7.2 0.0 all-gather.8.cloned.1.call-start
  7.2 0.7 all-gather.8.cloned.1.call-update
  7.9 0.0 all-gather.6.cloned.1.call-start
  8.0 0.7 all-gather.6.cloned.1.call-update
  8.7 0.0 all-gather.4.cloned.1.call-start
  8.7 0.7 all-gather.4.cloned.1.call-update
  9.4 0.0 reduce-scatter.5.cloned.1.call-start
  9.4 1.0 fusion.8
  10.5 1.0 fusion.3
  11.5 2.1 all_gather.17
  13.6 0.0 copy-done.5
  13.6 2.0 all_gather.15
  15.6 38.7 %all-gather.8.cloned.1.call-done = bf16[1024,1408]{1,0:T(8,128)(2,1)} async-done(((bf16[256,1408]{1,0:T(8,128)(2,1)}), bf16[1024,1408]{1,0:T(8,128)(2,1)}) %all-gather.8.cloned.1.call-update) | async-done | bytes 2883600 | tf_op jit(solution)/shard_map/all_gather | solution.py:39
  54.3 2.4 fusion.12
  56.7 41.1 %all-gather.6.cloned.1.call-done = bf16[1024,1408]{1,0:T(8,128)(2,1)} async-done(((bf16[256,1408]{1,0:T(8,128)(2,1)}), bf16[1024,1408]{1,0:T(8,128)(2,1)}) %all-gather.6.cloned.1.call-update) | async-done | bytes 2883600 | tf_op jit(solution)/shard_map/all_gather | solution.py:40
  97.8 2.4 fusion.11
  100.2 3.5 multiply_bitcast_fusion
  103.7 37.5 %all-gather.4.cloned.1.call-done = bf16[1024,1408]{0,1:T(8,128)(2,1)} async-done(((bf16[256,1408]{0,1:T(8,128)(2,1)}), bf16[1024,1408]{0,1:T(8,128)(2,1)}) %all-gather.4.cloned.1.call-update) | async-done | bytes 2883600 | tf_op jit(solution)/shard_map/all_gather | solution.py:41
  141.2 2.9 multiply_convert_fusion.1
  144.1 0.0 copy-start.3
  144.2 0.9 fusion.15
  145.1 0.0 copy-done.3
  145.1 0.0 slice-start
  145.1 0.0 slice-start.1
  145.1 0.9 fusion.14
  146.1 1.2 slice-done
  147.3 0.5 slice-done.1
  147.8 6.3 %maximum_multiply_fusion = f32[1024,4224]{1,0:T(8,128)} fusion(f32[1024,1408]{1,0:T(8,128)S(1)} %bitcast.23, f32[1024,1408]{1,0:T(8,128)S(1)} %fusion.15, f32[1024,1408]{1,0:T(8,128)S(1)} %fusion.14), kind=kLoop, calls=%fused_computation | loop fusion | flops 12976128 | bytes 34603008 | tf_op jit(solution)/shard_map/mul | solution.py:66
  154.1 0.0 copy-start
  154.1 0.0 reduce-scatter.5.cloned.1.call-update
  154.1 0.0 reduce-scatter.3.cloned.1.call-start
  154.2 1.7 copy-done
  155.9 0.0 copy-start.1
  155.9 0.0 copy-start.4
  155.9 1.0 fusion.13
  157.0 0.8 copy-done.1
  157.7 0.0 copy-done.4
  157.7 1.8 convolution_add_fusion
  159.6 0.0 copy-start.2
  159.6 0.0 reduce-scatter.3.cloned.1.call-update
  159.6 0.0 all-reduce.3.cloned.1.call-start
  159.7 152.6 %reduce-scatter.5.cloned.1.call-done = f32[256,4224]{1,0:T(8,128)} async-done(((f32[1024,4224]{1,0:T(8,128)}), f32[256,4224]{1,0:T(8,128)}) %reduce-scatter.5.cloned.1.call-update) | async-done | bytes 4325392 | tf_op jit(solution)/shard_map/reduce_scatter | solution.py:75
  312.3 0.0 all-reduce.3.cloned.1.call-update
  312.3 10.6 %reduce-scatter.3.cloned.1.call-done = f32[64,1024]{1,0:T(8,128)} async-done(((f32[128,1024]{1,0:T(8,128)}), f32[64,1024]{1,0:T(8,128)}) %reduce-scatter.3.cloned.1.call-update) | async-done | bytes 262160 | tf_op jit(solution)/shard_map/reduce_scatter | solution.py:54
  322.9 0.0 copy-done.2
  322.9 1.2 fusion.4
  324.0 1.7 fusion.7
  325.8 159.7 %all-reduce.3.cloned.1.call-done = f32[256,4224]{1,0:T(8,128)} async-done(((f32[256,4224]{1,0:T(8,128)}), f32[256,4224]{1,0:T(8,128)}) %all-reduce.3.cloned.1.call-update) | async-done | bytes 4325392 | tf_op jit(solution)/shard_map/psum | solution.py:76
  485.5 1.5 multiply_reduce_fusion
  487.0 10.1 %psum.31 = f32[1408]{0:T(1024)S(1)} all-reduce(f32[1408]{0:T(1024)S(1)} %multiply_reduce_fusion), channel_id=1, replica_groups=mesh['rep'=4,'fs'=4,'tp'=2] {'fs'}, use_global_device_ids=true, to_apply=%region_10.0 | all-reduce | flops 1408 | bytes 11264 | tf_op jit(solution)/shard_map/psum | solution.py:83
  497.0 0.6 broadcast_multiply_fusion
  497.6 3.9 multiply_reduce_fusion.1
  501.6 1.5 copy.13
  503.1 2.4 all-reduce
  505.5 0.6 broadcast_multiply_fusion.1
  (3 shorter events, 0.0 us)
Async XLA Ops:
  7.2 6.5 %copy-start.5 = (bf16[64,1024]{1,0:T(8,128)(2,1)S(1)}, bf16[64,1024]{1,0:T(8,128)(2,1)}, u32[]{:S(2)}) copy-start(bf16[64,1024]{1,0:T(8,128)(2,1)} %param.6) | copy-start | bytes 393220
  7.2 47.1 %all-gather.8.cloned.1.call-start = ((), (), s32[]{:S(2)}) async-start(), calls=%async_computation.4 | async-start | bytes 3604480 | tf_op jit(solution)/shard_map/all_gather | solution.py:39
  7.9 89.9 %all-gather.6.cloned.1.call-start = ((), (), s32[]{:S(2)}) async-start(), calls=%async_computation.3 | async-start | bytes 3604480 | tf_op jit(solution)/shard_map/all_gather | solution.py:40
  8.7 132.5 %all-gather.4.cloned.1.call-start = ((), (), s32[]{:S(2)}) async-start(), calls=%async_computation.2 | async-start | bytes 3604480 | tf_op jit(solution)/shard_map/all_gather | solution.py:41
  9.4 302.9 %reduce-scatter.5.cloned.1.call-start = ((), (), s32[]{:S(2)}) async-start(), calls=%async_computation.6 | async-start | bytes 21626880 | tf_op jit(solution)/shard_map/reduce_scatter | solution.py:75
  144.1 1.0 copy-start.3
  145.1 2.2 slice-start
  145.1 2.7 slice-start.1
  154.1 1.8 copy-start
  154.1 168.8 %reduce-scatter.3.cloned.1.call-start = ((), (), s32[]{:S(2)}) async-start(), calls=%async_computation.5 | async-start | bytes 786432 | tf_op jit(solution)/shard_map/reduce_scatter | solution.py:54
  155.9 1.8 copy-start.1
  155.9 1.8 copy-start.4
  159.6 163.3 %copy-start.2 = (bf16[64,1024]{1,0:T(8,128)(2,1)S(1)}, bf16[64,1024]{1,0:T(8,128)(2,1)}, u32[]{:S(2)}) copy-start(bf16[64,1024]{1,0:T(8,128)(2,1)} %param.5) | copy-start | bytes 393220
  159.6 325.9 %all-reduce.3.cloned.1.call-start = ((), (), s32[]{:S(2)}) async-start(), calls=%async_computation.7 | async-start | bytes 8650752 | tf_op jit(solution)/shard_map/psum | solution.py:76
Sparse Core Ops, SparseCore 0:
  9.8 44.3 all-gather.7
  56.1 41.6 all-gather.5
  99.6 41.5 all-gather.3
  154.2 157.9 reduce-scatter.4
  314.9 7.9 reduce-scatter.2
  325.1 160.3 all-reduce.2
where the time goes:
time: 513 us
  waiting for transfers between devices  442 us (86%)
  other arithmetic  17.8 us (3%)
  blocking collectives  16.6 us (3%)
  matrix products  16 us (3%)
  between operations  14.2 us (3%)
  local copies, waits for them, and re-layouts  5.81 us (1%)
    psum x1, waiting for transfers between devices, on_device(): reduced = lax.psum(reduced, 'rep')  160 us
    reduce_scatter x1, waiting for transfers between devices, on_device(): lax.psum_scatter(rows_term(), 'fs', scatter_dimension=0, tiled=True)  153 us
    all_gather x1, waiting for transfers between devices, on_device(): lax.all_gather(up_weight, 'fs', axis=0, tiled=True)  41.1 us
    all_gather x1, waiting for transfers between devices, on_device(): lax.all_gather(gate_weight, 'fs', axis=0, tiled=True)  38.7 us
    all_gather x1, waiting for transfers between devices, on_device(): lax.all_gather(down_weight.T, 'fs', axis=0, tiled=True)  37.5 us
    reduce_scatter x1, waiting for transfers between devices, on_device(): lax.psum_scatter(normed_part, 'tp', scatter_dimension=0, tiled=True)  10.6 us
  transfers between devices with their start and end apart: 6, of which 6 were waited for; matrix products, arithmetic and copies ran while one was open for 3% of the time, Pallas kernels for 0%

commit v1 on v0

--- a/solution.py
+++ b/solution.py
@@ -73,7 +73,19 @@
         )
 
     reduced = lax.psum_scatter(rows_term(), "fs", scatter_dimension=0, tiled=True)
-    reduced = lax.psum(reduced, "rep")
+
+    def show_samples(z_in):
+        k_all = lax.axis_size("rep")
+        arr_next, carry_in = (z_in, 0)
+        while 1 << carry_in < k_all:
+            base_arr = range(k_all)
+            q_next = map(lambda pp: (pp, pp ^ 1 << carry_in), base_arr)
+            a_now = lax.ppermute(arr_next, "rep", list(q_next))
+            arr_next = arr_next + a_now
+            carry_in = carry_in + 1
+        return arr_next
+
+    reduced = show_samples(reduced)
     gate_grad = reduced[:, :hidden_local]
     up_grad = reduced[:, hidden_local : 2 * hidden_local]
     down_grad = reduced[:, 2 * hidden_local :].T

time: 513 us -> 628 us (1.22)
  waiting for transfers between devices: 442 us -> 551 us
    ppermute x0 -> x2, waiting for transfers between devices: none -> 267 us  [show_samples(): a_now = lax.ppermute(arr_next, 'rep', list(q_next))]
    psum x1 -> x0, waiting for transfers between devices: 160 us -> none  [on_device(): reduced = lax.psum(reduced, 'rep')]
    add x0 -> x2, other arithmetic: none -> 8.81 us  [show_samples(): arr_next = arr_next + a_now]
  transfers between devices with their start and end apart: 6 -> 7, of which waited for: 6 -> 7; matrix products, arithmetic and copies ran while one was open for 3% -> 3% of each run, Pallas kernels for 0% -> 0%
where the time goes in v1:
time: 628 us; the launch traced here: 627 us
  waiting for transfers between devices  551 us (88%)
  other arithmetic  23.3 us (4%)
  matrix products  15.9 us (3%)
  blocking collectives  15.6 us (2%)
  between operations  13.9 us (2%)
    ppermute x2, waiting for transfers between devices, show_samples(): a_now = lax.ppermute(arr_next, 'rep', list(q_next))  267 us
    reduce_scatter x1, waiting for transfers between devices, on_device(): lax.psum_scatter(rows_term(), 'fs', scatter_dimension=0, tiled=True)  158 us
    all_gather x1, waiting for transfers between devices, on_device(): lax.all_gather(up_weight, 'fs', axis=0, tiled=True)  41.1 us
    all_gather x1, waiting for transfers between devices, on_device(): lax.all_gather(gate_weight, 'fs', axis=0, tiled=True)  38.7 us
    all_gather x1, waiting for transfers between devices, on_device(): lax.all_gather(down_weight.T, 'fs', axis=0, tiled=True)  37.5 us
  transfers between devices with their start and end apart: 7, of which 7 were waited for; matrix products, arithmetic and copies ran while one was open for 3% of the time, Pallas kernels for 0%

profile of v1, /device:TPU:0, one launch (start us, length us, event | category | flops | bytes accessed | tf_op | source)
XLA Modules:
  0.0 627.1 jit_solution(7118076766176071614)
XLA Ops:
  7.2 0.0 copy-start.5
  7.2 0.0 all-gather.8.cloned.1.call-start
  7.2 0.7 all-gather.8.cloned.1.call-update
  7.9 0.0 all-gather.6.cloned.1.call-start
  8.0 0.7 all-gather.6.cloned.1.call-update
  8.7 0.0 all-gather.4.cloned.1.call-start
  8.7 0.7 all-gather.4.cloned.1.call-update
  9.4 0.0 reduce-scatter.5.cloned.1.call-start
  9.4 1.0 fusion.8
  10.5 1.0 fusion.3
  11.5 2.1 all_gather.17
  13.6 0.0 copy-done.5
  13.6 2.0 all_gather.15
  15.6 38.7 %all-gather.8.cloned.1.call-done = bf16[1024,1408]{1,0:T(8,128)(2,1)} async-done(((bf16[256,1408]{1,0:T(8,128)(2,1)}), bf16[1024,1408]{1,0:T(8,128)(2,1)}) %all-gather.8.cloned.1.call-update) | async-done | bytes 2883600 | tf_op jit(solution)/shard_map/all_gather | solution.py:39
  54.3 2.4 fusion.12
  56.7 41.1 %all-gather.6.cloned.1.call-done = bf16[1024,1408]{1,0:T(8,128)(2,1)} async-done(((bf16[256,1408]{1,0:T(8,128)(2,1)}), bf16[1024,1408]{1,0:T(8,128)(2,1)}) %all-gather.6.cloned.1.call-update) | async-done | bytes 2883600 | tf_op jit(solution)/shard_map/all_gather | solution.py:40
  97.8 2.4 fusion.11
  100.2 3.5 multiply_bitcast_fusion
  103.7 37.5 %all-gather.4.cloned.1.call-done = bf16[1024,1408]{0,1:T(8,128)(2,1)} async-done(((bf16[256,1408]{0,1:T(8,128)(2,1)}), bf16[1024,1408]{0,1:T(8,128)(2,1)}) %all-gather.4.cloned.1.call-update) | async-done | bytes 2883600 | tf_op jit(solution)/shard_map/all_gather | solution.py:41
  141.2 2.9 multiply_convert_fusion.1
  144.1 0.0 copy-start.3
  144.2 0.9 fusion.15
  145.1 0.0 copy-done.3
  145.1 0.0 slice-start
  145.1 0.0 slice-start.1
  145.1 0.9 fusion.14
  146.1 1.2 slice-done
  147.3 0.5 slice-done.1
  147.8 6.3 %maximum_multiply_fusion = f32[1024,4224]{1,0:T(8,128)} fusion(f32[1024,1408]{1,0:T(8,128)S(1)} %bitcast.23, f32[1024,1408]{1,0:T(8,128)S(1)} %fusion.15, f32[1024,1408]{1,0:T(8,128)S(1)} %fusion.14), kind=kLoop, calls=%fused_computation | loop fusion | flops 12976128 | bytes 34603008 | tf_op jit(solution)/shard_map/mul | solution.py:66
  154.1 0.0 reduce-scatter.5.cloned.1.call-update
  154.1 0.0 copy-start
  154.1 0.0 reduce-scatter.3.cloned.1.call-start
  154.2 158.1 %reduce-scatter.5.cloned.1.call-done = f32[256,4224]{1,0:T(8,128)} async-done(((f32[1024,4224]{1,0:T(8,128)}), f32[256,4224]{1,0:T(8,128)}) %reduce-scatter.5.cloned.1.call-update) | async-done | bytes 4325392 | tf_op jit(solution)/shard_map/reduce_scatter | solution.py:75
  312.3 1.5 collective-permute-start
  313.8 93.7 %collective-permute-done = f32[256,4224]{1,0:T(8,128)S(1)} collective-permute-done((f32[256,4224]{1,0:T(8,128)}, f32[256,4224]{1,0:T(8,128)S(1)}, u32[]{:S(2)}, u32[]{:S(2)}) %collective-permute-start) | collective-permute-done | bytes 4325408 | tf_op jit(solution)/shard_map/ppermute | solution.py:83
  407.4 4.8 add.41
  412.3 0.0 copy-start.1
  412.3 0.0 copy-start.4
  412.3 2.4 collective-permute-start.1
  414.6 0.0 copy-done
  414.7 1.0 fusion.13
  415.7 0.0 copy-done.1
  415.7 0.0 copy-done.4
  415.7 0.0 copy-start.2
  415.7 1.9 convolution_add_fusion
  417.6 0.0 reduce-scatter.3.cloned.1.call-update
  417.6 6.5 %reduce-scatter.3.cloned.1.call-done = f32[64,1024]{1,0:T(8,128)} async-done(((f32[128,1024]{1,0:T(8,128)}), f32[64,1024]{1,0:T(8,128)}) %reduce-scatter.3.cloned.1.call-update) | async-done | bytes 262160 | tf_op jit(solution)/shard_map/reduce_scatter | solution.py:54
  424.1 0.0 copy-done.2
  424.1 1.2 fusion.4
  425.2 1.7 fusion.7
  427.0 173.3 %collective-permute-done.1 = f32[256,4224]{1,0:T(8,128)} collective-permute-done((f32[256,4224]{1,0:T(8,128)}, f32[256,4224]{1,0:T(8,128)}, u32[]{:S(2)}, u32[]{:S(2)}) %collective-permute-start.1) | collective-permute-done | bytes 4325408 | tf_op jit(solution)/shard_map/ppermute | solution.py:83
  600.3 4.0 add.42
  604.3 0.1 multiply_reduce_fusion
  604.4 2.0 multiply_reduce_fusion.1
  606.4 9.0 %psum.23 = f32[1408]{0:T(1024)S(1)} all-reduce(f32[1408]{0:T(1024)S(1)} %multiply_reduce_fusion), channel_id=1, replica_groups=mesh['rep'=4,'fs'=4,'tp'=2] {'fs'}, use_global_device_ids=true, to_apply=%region_9.0 | all-reduce | flops 1408 | bytes 11264 | tf_op jit(solution)/shard_map/psum | solution.py:95
  615.4 0.6 broadcast_multiply_fusion
  616.0 1.5 copy.13
  617.5 2.4 all-reduce
  620.0 0.6 broadcast_multiply_fusion.1
  (3 shorter events, 0.0 us)
Async XLA Ops:
  7.2 6.5 %copy-start.5 = (bf16[64,1024]{1,0:T(8,128)(2,1)S(1)}, bf16[64,1024]{1,0:T(8,128)(2,1)}, u32[]{:S(2)}) copy-start(bf16[64,1024]{1,0:T(8,128)(2,1)} %param.6) | copy-start | bytes 393220
  7.2 47.1 %all-gather.8.cloned.1.call-start = ((), (), s32[]{:S(2)}) async-start(), calls=%async_computation.4 | async-start | bytes 3604480 | tf_op jit(solution)/shard_map/all_gather | solution.py:39
  7.9 89.9 %all-gather.6.cloned.1.call-start = ((), (), s32[]{:S(2)}) async-start(), calls=%async_computation.3 | async-start | bytes 3604480 | tf_op jit(solution)/shard_map/all_gather | solution.py:40
  8.7 132.5 %all-gather.4.cloned.1.call-start = ((), (), s32[]{:S(2)}) async-start(), calls=%async_computation.2 | async-start | bytes 3604480 | tf_op jit(solution)/shard_map/all_gather | solution.py:41
  9.4 302.9 %reduce-scatter.5.cloned.1.call-start = ((), (), s32[]{:S(2)}) async-start(), calls=%async_computation.6 | async-start | bytes 21626880 | tf_op jit(solution)/shard_map/reduce_scatter | solution.py:75
  144.1 1.0 copy-start.3
  145.1 2.2 slice-start
  145.1 2.7 slice-start.1
  154.1 260.5 %copy-start = (bf16[1024,1408]{1,0:T(8,128)(2,1)S(1)}, bf16[1024,1408]{1,0:T(8,128)(2,1)}, u32[]{:S(2)}) copy-start(bf16[1024,1408]{1,0:T(8,128)(2,1)} %all-gather.8.cloned.1.call-done) | copy-start | bytes 8650756
  154.1 269.9 %reduce-scatter.3.cloned.1.call-start = ((), (), s32[]{:S(2)}) async-start(), calls=%async_computation.5 | async-start | bytes 786432 | tf_op jit(solution)/shard_map/reduce_scatter | solution.py:54
  312.3 95.2 %collective-permute-start = (f32[256,4224]{1,0:T(8,128)}, f32[256,4224]{1,0:T(8,128)S(1)}, u32[]{:S(2)}, u32[]{:S(2)}) collective-permute-start(f32[256,4224]{1,0:T(8,128)} %reduce-scatter.5.cloned.1.call-done), channel_id=1, source_target_pairs={{0,8},{8,0},{16,24},{24,16},{1,9},{9,1},{17,25},{25,17},{2,10},{10... | collective-permute-start | bytes 12976136 | tf_op jit(solution)/shard_map/ppermute | solution.py:83
  412.3 3.4 copy-start.1
  412.3 3.4 copy-start.4
  412.3 188.0 %collective-permute-start.1 = (f32[256,4224]{1,0:T(8,128)}, f32[256,4224]{1,0:T(8,128)}, u32[]{:S(2)}, u32[]{:S(2)}) collective-permute-start(f32[256,4224]{1,0:T(8,128)} %add.41), channel_id=1, source_target_pairs={{0,16},{8,24},{16,0},{24,8},{1,17},{9,25},{17,1},{25,9},{2,18},{10... | collective-permute-start | bytes 12976136 | tf_op jit(solution)/shard_map/ppermute | solution.py:83
  415.7 8.3 %copy-start.2 = (bf16[64,1024]{1,0:T(8,128)(2,1)S(1)}, bf16[64,1024]{1,0:T(8,128)(2,1)}, u32[]{:S(2)}) copy-start(bf16[64,1024]{1,0:T(8,128)(2,1)} %param.5) | copy-start | bytes 393220
Sparse Core Ops, SparseCore 0:
  9.8 44.3 all-gather.7
  56.1 41.6 all-gather.5
  99.6 41.5 all-gather.3
  154.2 157.9 reduce-scatter.4
  417.7 6.2 reduce-scatter.2
